TPU v7x, 512 devices: a whole 4x4x16 slice. The times are simulated.
512 devices in a mesh: fs: 64 (over z, y), tp: 8 (over x, core).
Axes of the slice: x: 4, y: 4, z: 16, core: 2. Of those that a mesh axis runs over, the one named last changes fastest.
Arguments:
- fwd_input: bfloat16 [8192, 2048], P('fs'), may hold values from -6 to 6
- saved_input: bfloat16 [8192, 2048], P('fs'), may hold values from -16 to 16
- out_cotangent: bfloat16 [8192, 2048], P('fs'), may hold values from -16 to 16
- up_weight: bfloat16 [2048, 4096], P('fs', 'tp'), may hold values from -0.125 to 0.125
- down_weight: bfloat16 [4096, 2048], P('tp', 'fs'), may hold values from -0.09375 to 0.09375
- up_grad_sum: float32 [2048, 4096], P('fs', 'tp'), may hold values from -6 to 6
Outputs:
- layer_out: bfloat16 [8192, 2048], P('fs')
- input_grad: bfloat16 [8192, 2048], P('fs')
- up_grad_out: float32 [2048, 4096], P('fs', 'tp')
All inputs are finite; a program needn't handle non-finite values.
Results may differ from a plain program's by a relative error of at most 0.013.
Values may be sent and summed in bfloat16 or wider, within the bound.
A program may use at most 64 MiB of HBM per device.

v0:
```python
import functools

import jax
import jax.numpy as jnp
from jax import lax
from jax.experimental import pallas as pl
from jax.experimental.pallas import tpu as pltpu
from jax.sharding import PartitionSpec as P

MESH = pl.DeviceIdType.MESH
F32 = jnp.float32
BF16 = jnp.bfloat16
PART = 256


def remote(src, dst, send_sem, recv_sem, fs, tp):
    return pltpu.make_async_remote_copy(
        src_ref=src,
        dst_ref=dst,
        send_sem=send_sem,
        recv_sem=recv_sem,
        device_id=(fs, tp),
        device_id_type=MESH,
    )


def kernel(
    n, T, B, Q, fwd, saved, cot, up, down, out, ing, gout,
    X, W, turned, H, O, tp_in, S, pl_in, G, from_left, from_right,
    lsem, wS, wR, zS, zR, aS, aR, bS, bR, tS, tR, pS, pR, fS, fR, gS, gL, gR, hS, hR,
):
    A = n // B
    f, t = lax.axis_index("fs"), lax.axis_index("tp")
    z, p = lax.div(f, B), lax.rem(f, B)
    far = A - 1 - z
    rows, D = fwd.shape
    C = rows // T
    Rw, F = up.shape
    Fs = F // B
    wide = Fs // Q
    tokens = B * rows
    peers = [lax.rem(p + i, B) for i in range(1, B)]
    mates = [lax.rem(t + i, T) for i in range(1, T)]
    has_left, has_right = z > 0, z < A - 1

    def chunk(index):
        return pl.ds(pl.multiple_of(index * C, C), C)

    def cols(index, c):
        return pl.ds(pl.multiple_of(index * Fs + c * wide, wide), wide)

    barrier = pltpu.get_barrier_semaphore()
    for q in peers:
        pl.semaphore_signal(barrier, inc=1, device_id=(z * B + q, t), device_id_type=MESH)
    for m in mates:
        pl.semaphore_signal(barrier, inc=1, device_id=(f, m), device_id_type=MESH)

    @pl.when(has_left)
    def _():
        pl.semaphore_signal(barrier, inc=1, device_id=(f - B, t), device_id_type=MESH)

    @pl.when(has_right)
    def _():
        pl.semaphore_signal(barrier, inc=1, device_id=(f + B, t), device_id_type=MESH)

    ends = lax.div(z + A - 1, A) + lax.div(far + A - 1, A)
    pl.semaphore_wait(barrier, B - 1 + T - 1 + ends)

    weights = (up, down if down.shape == up.shape else turned)

    def slice_out(c, pc, i, q):
        return remote(
            weights[pc].at[:, cols(q, c)], W.at[c, pc, f], wS.at[c, pc, i], wR.at[c, pc, p], z * B + q, t
        )

    def slice_in(c, pc, q):
        there = W.at[c, pc, z * B + q]
        return remote(there, there, wS.at[c, pc, 0], wR.at[c, pc, q], z * B + q, t)

    def line(c, pc, k, q, way, src=None):
        at = k * B + q
        block = W.at[c, pc, at]
        target = f + B if way == 0 else f - B
        return remote(
            block if src is None else src, block, zS.at[way, c, pc, at], zR.at[c, pc, at], target, t
        )

    def own_out(c, pc, q, way):
        src = weights[pc].at[:, cols(p, c)] if q is p else None
        line(c, pc, z, q, way, src).start()

    def both_ways(c, pc, q):
        @pl.when(has_right)
        def _():
            own_out(c, pc, q, 0)

        @pl.when(has_left)
        def _():
            own_out(c, pc, q, 1)

    own_w = [
        pltpu.make_async_copy(weights[pc].at[:, cols(p, c)], W.at[c, pc, f], lsem.at[3 + 2 * c + pc])
        for c in range(Q) for pc in range(2)
    ]
    for c in range(Q):
        for pc in range(2):
            if (c, pc) == (0, 1) and weights[1] is turned:
                turned[...] = down[...].T
            for i, q in enumerate(peers):
                slice_out(c, pc, i, q).start()
            if c == 0:
                both_ways(c, pc, p)
    for copy in own_w:
        copy.start()

    acts = (fwd, saved, cot)

    def act_out(j, i, q):
        return remote(acts[j].at[chunk(t)], X.at[j, p, chunk(t)], aS.at[j, i], aR.at[j, p], z * B + q, t)

    def act_in(j, q):
        there = X.at[j, q, chunk(t)]
        return remote(there, there, aS.at[j, 0], aR.at[j, q], z * B + q, t)

    own_x = [pltpu.make_async_copy(acts[j], X.at[j, p], lsem.at[j]) for j in range(3)]
    for j in (1, 2, 0):
        own_x[j].start()
        for i, q in enumerate(peers):
            act_out(j, i, q).start()

    def act_share(i, q, o, m):
        there = X.at[:, q, chunk(t)]
        return remote(there, there, bS.at[i, o], bR.at[q, t], f, m)

    def act_shared(i, q, o, m):
        there = X.at[:, q, chunk(m)]
        return remote(there, there, bS.at[i, o], bR.at[q, m], f, m)

    for pc in range(2):
        for q in peers:
            slice_in(0, pc, q).wait_recv()
            both_ways(0, pc, q)

    order = [p] + peers

    def gather_step(c, s):
        for pc in range(2):
            for q in order:

                @pl.when(z >= s)
                def _(pc=pc, q=q):
                    line(c, pc, z - s, q, 0).wait_recv()

                    @pl.when(has_right)
                    def _():
                        line(c, pc, z - s, q, 0).start()

                @pl.when(far >= s)
                def _(pc=pc, q=q):
                    line(c, pc, z + s, q, 1).wait_recv()

                    @pl.when(has_left)
                    def _():
                        line(c, pc, z + s, q, 1).start()

        if c == 0 and s == 1:
            for later in range(1, Q):
                for pc in range(2):
                    for q in peers:
                        slice_in(later, pc, q).wait_recv()
        if c + 1 < Q:
            @pl.when(jnp.logical_and(has_right, z == s if s > 1 else z <= 1))
            def _():
                for pc in range(2):
                    for q in order:
                        own_out(c + 1, pc, q, 0)

            @pl.when(jnp.logical_and(has_left, far == s if s > 1 else far <= 1))
            def _():
                for pc in range(2):
                    for q in order:
                        own_out(c + 1, pc, q, 1)

        if c == 0 and s == max(A - 2, 1):
            for i, q in enumerate(peers):
                for j in range(3):
                    act_in(j, q).wait_recv()
                for o, m in enumerate(mates):
                    act_share(i, q, o, m).start()

    def product(c, j, pc):
        return jnp.dot(
            X[j].reshape(tokens, D), W[c, pc].reshape(D, wide), preferred_element_type=F32
        )

    def to_right(c, d):
        return remote(G.at[c, d], from_left.at[c, d], gS.at[c, d], gL.at[c, d], f + B, t)

    def to_left(c, d):
        return remote(G.at[c, d], from_right.at[c, d], gS.at[c, d], gR.at[c, d], f - B, t)

    def add_left(c, d):
        remote(from_left.at[c, d], from_left.at[c, d], gS.at[c, d], gL.at[c, d], f - B, t).wait_recv()
        G[c, d] = (G[c, d].astype(F32) + from_left[c, d].astype(F32)).astype(BF16)

    def add_right(c, d):
        remote(from_right.at[c, d], from_right.at[c, d], gS.at[c, d], gR.at[c, d], f + B, t).wait_recv()
        G[c, d] = (G[c, d].astype(F32) + from_right[c, d].astype(F32)).astype(BF16)

    def grad_out(c, i, q):
        return remote(G.at[c, z, q], gout.at[:, cols(p, c)], hS.at[c, i], hR.at[c, p], z * B + q, t)

    def sum_step(c, s):
        if s < A - 1:

            @pl.when(jnp.logical_and(has_left, z <= s))
            def _():
                add_left(c, far - s + 2 * z)
                to_right(c, far - s + 2 * z).start()

            @pl.when(jnp.logical_and(has_right, far <= s))
            def _():
                add_right(c, s - far)
                to_left(c, s - far).start()

        else:

            @pl.when(has_left)
            def _():
                add_left(c, z)

            @pl.when(has_right)
            def _():
                add_right(c, z)

            for i, q in enumerate(peers):
                grad_out(c, i, q).start()
            gout[:, cols(p, c)] = G[c, z, p]

    planes = []
    for i in range((A + 1) // 2):
        planes += [A - 1 - i] if A - 1 - i == i else [A - 1 - i, i]
    deep = B * Rw

    def backward(c):
        pre = product(c, 1, 0)
        d_hidden = product(c, 2, 1)
        H[1, c] = (d_hidden * 2.0 * jnp.maximum(pre, 0.0)).astype(BF16)
        for d in planes:
            term = lax.dot_general(
                X[1, :, :, d * deep:(d + 1) * deep].reshape(tokens, deep),
                H[1, c],
                (((0,), (0,)), ((), ())),
                preferred_element_type=F32,
            )
            G[c, d] = term.astype(BF16).reshape(B, Rw, wide)
            if d > 0:

                @pl.when(z == 0)
                def _(d=d):
                    to_right(c, d).start()

            if d < A - 1:

                @pl.when(far == 0)
                def _(d=d):
                    to_left(c, d).start()

    def forward(c):
        positive = jnp.maximum(product(c, 0, 0), 0.0)
        H[0, c] = (positive * positive).astype(BF16)

    for c in range(Q):
        for s in range(1, A):
            gather_step(c, s)
            if c > 0:
                sum_step(c - 1, s)
        if c == 0:
            for copy in own_w + own_x:
                copy.wait()
            for i, q in enumerate(peers):
                for o, m in enumerate(mates):
                    act_shared(i, q, o, m).wait_recv()
        backward(c)
        if c + 1 < Q:
            forward(c)

    pack = max(1, 256 // Rw)

    def spread(o, pc):
        @pl.loop(0, n // pack)
        def _(g):
            part = 0.0
            for c in range(Q):
                block = W[c, pc, pl.ds(g * pack, pack)].reshape(pack * Rw, wide)
                part += lax.dot_general(
                    H[o, c], block, (((1,), (1,)), ((), ())), preferred_element_type=F32
                )
            at = pl.ds(pl.multiple_of(g * (pack * Rw), pack * Rw), pack * Rw)
            O[o, :, :, at] = part.astype(BF16).reshape(B, rows, pack * Rw)

    def tp_out(o, i, m):
        return remote(O.at[o, :, chunk(m)], tp_in.at[o, t], tS.at[o, i], tR.at[o, t], f, m)

    def tp_got(o, i, m):
        return remote(tp_in.at[o, m], tp_in.at[o, m], tS.at[o, i], tR.at[o, m], f, m)

    def plane_out(o, i, q):
        return remote(S.at[o, q], pl_in.at[o, p], pS.at[o, i], pR.at[o, p], z * B + q, t)

    def plane_got(o, i, q):
        return remote(pl_in.at[o, q], pl_in.at[o, q], pS.at[o, i], pR.at[o, q], z * B + q, t)

    def plane_sums(o):
        for i, m in enumerate(mates):
            tp_got(o, i, m).wait_recv()
        for i, q in enumerate(peers + [p]):
            total = O[o, q, chunk(t)].astype(F32)
            for m in mates:
                total = total + tp_in[o, m, q].astype(F32)
            S[o, q] = total.astype(BF16)
            if i < len(peers):
                plane_out(o, i, q).start()

    spread(1, 0)
    for i, m in enumerate(mates):
        tp_out(1, i, m).start()
    forward(Q - 1)
    plane_sums(1)
    spread(0, 1)
    for i, m in enumerate(mates):
        tp_out(0, i, m).start()
    plane_sums(0)
    for s in range(1, A):
        sum_step(Q - 1, s)

    outs = (out, ing)

    def share(o, i, m):
        there = outs[o].at[chunk(t)]
        return remote(there, there, fS.at[o, i], fR.at[o, t], f, m)

    def shared(o, i, m):
        there = outs[o].at[chunk(m)]
        return remote(there, there, fS.at[o, i], fR.at[o, m], f, m)

    for o in (1, 0):
        total = S[o, p].astype(F32)
        for i, q in enumerate(peers):
            plane_got(o, i, q).wait_recv()
            total = total + pl_in[o, q].astype(F32)
        outs[o][chunk(t)] = total.astype(BF16)
        for i, m in enumerate(mates):
            share(o, i, m).start()

    for i, q in enumerate(peers):
        for c in range(Q):
            there = gout.at[:, cols(q, c)]
            remote(there, there, hS.at[c, i], hR.at[c, q], z * B + q, t).wait_recv()
            grad_out(c, i, q).wait_send()
            for pc in range(2):
                slice_out(c, pc, i, q).wait_send()
        for j in range(3):
            act_out(j, i, q).wait_send()
        for o, m in enumerate(mates):
            act_share(i, q, o, m).wait_send()
        for o in range(2):
            plane_out(o, i, q).wait_send()
    for i, m in enumerate(mates):
        for o in range(2):
            tp_out(o, i, m).wait_send()
            share(o, i, m).wait_send()
            shared(o, i, m).wait_recv()
    for s in range(A):

        @pl.when(jnp.logical_and(has_right, z >= s))
        def _(s=s):
            for c in range(Q):
                for pc in range(2):
                    for q in range(B):
                        line(c, pc, z - s, q, 0).wait_send()

        @pl.when(jnp.logical_and(has_left, far >= s))
        def _(s=s):
            for c in range(Q):
                for pc in range(2):
                    for q in range(B):
                        line(c, pc, z + s, q, 1).wait_send()

    for d in range(A):
        for c in range(Q):

            @pl.when(z < d)
            def _(c=c, d=d):
                to_right(c, d).wait_send()

            @pl.when(z > d)
            def _(c=c, d=d):
                to_left(c, d).wait_send()


def groups(n, width):
    size = 1
    while 4 * size * size <= n and n % (2 * size) == 0 and width // (2 * size) >= 128:
        size *= 2
    return size


def per_device(n, T, fwd_input, saved_input, out_cotangent, up_weight, down_weight, up_grad_sum):
    rows, D = fwd_input.shape
    Rw, F = up_weight.shape
    B = groups(n, F)
    A, Fs, C = n // B, F // B, rows // T
    Q = max(1, Fs // PART)
    wide = Fs // Q
    down = down_weight if Rw % 128 == 0 and down_weight.shape != up_weight.shape else down_weight.T
    dma = pltpu.SemaphoreType.DMA
    side, mate = max(B - 1, 1), max(T - 1, 1)
    flops = 12 * B * rows * Fs * D
    vmem = pl.BlockSpec(memory_space=pltpu.VMEM)
    layer_out, input_grad, grad = pl.pallas_call(
        functools.partial(kernel, n, T, B, Q),
        out_shape=(
            jax.ShapeDtypeStruct((rows, D), BF16),
            jax.ShapeDtypeStruct((rows, D), BF16),
            jax.ShapeDtypeStruct((Rw, F), BF16),
        ),
        in_specs=[vmem] * 5,
        out_specs=(vmem,) * 3,
        scratch_shapes=[
            pltpu.VMEM((3, B, rows, D), BF16),
            pltpu.VMEM((Q, 2, n, Rw, wide), BF16),
            pltpu.VMEM((Rw, F), BF16),
            pltpu.VMEM((2, Q, B * rows, wide), BF16),
            pltpu.VMEM((2, B, rows, D), BF16),
            pltpu.VMEM((2, T, B, C, D), BF16),
            pltpu.VMEM((2, B, C, D), BF16),
            pltpu.VMEM((2, B, C, D), BF16),
            pltpu.VMEM((Q, A, B, Rw, wide), BF16),
            pltpu.VMEM((Q, A, B, Rw, wide), BF16),
            pltpu.VMEM((Q, A, B, Rw, wide), BF16),
            dma((3 + 2 * Q,)),
            dma((Q, 2, side)), dma((Q, 2, B)),
            dma((2, Q, 2, n)), dma((Q, 2, n)),
            dma((3, side)), dma((3, B)),
            dma((side, mate)), dma((B, T)),
            dma((2, mate)), dma((2, T)),
            dma((2, side)), dma((2, B)),
            dma((2, mate)), dma((2, T)),
            dma((Q, A)), dma((Q, A)), dma((Q, A)),
            dma((Q, side)), dma((Q, B)),
        ],
        compiler_params=pltpu.CompilerParams(
            collective_id=0, has_side_effects=True, vmem_limit_bytes=58 * 2**20
        ),
        cost_estimate=pl.CostEstimate(flops=flops, bytes_accessed=2**25, transcendentals=0),
    )(fwd_input, saved_input, out_cotangent, up_weight, down)
    grad_part = grad.astype(F32)
    grad_scale = float(rows * n) ** (-0.5)
    return (layer_out, input_grad, up_grad_sum + grad_part * grad_scale)


def solution(mesh):
    placed = (
        P("fs", None),
        P("fs", None),
        P("fs", None),
        P("fs", "tp"),
        P("tp", "fs"),
        P("fs", "tp"),
    )
    return jax.shard_map(
        functools.partial(per_device, mesh.shape["fs"], mesh.shape["tp"]),
        mesh=mesh,
        in_specs=placed,
        out_specs=(P("fs", None), P("fs", None), P("fs", "tp")),
        check_vma=False,
    )
```

profile of v0, /device:TPU:1, one launch (start us, length us, event | category | flops | bytes accessed | tf_op | source)
XLA Modules:
  0.0 221.1 jit_solution(5250448584245595964)
XLA Ops:
  0.6 0.0 copy-start.1
  0.6 216.3 %shard_map.85 = (bf16[128,2048]{1,0:T(8,128)(2,1)}, bf16[128,2048]{1,0:T(8,128)(2,1)}, bf16[32,512]{1,0:T(8,128)(2,1)}) custom-call(bf16[128,2048]{1,0:T(8,128)(2,1)} %fwd.1, bf16[128,2048]{1,0:T(8,128)(2,1)} %saved.1, bf16[128,2048]{1,0:T(8,128)(2,1)} %cot.1, bf16[32,512]{1,0:T(8,128)(2,1)} %up.1, bf16[32,512]{1,0:T(8,128)(2,1)} %bitcast.1), custom_call_target="tpu_custom_call" | custom-call | flops 1610612736 | bytes 33554432 | tf_op jit(solution)/shard_map/pallas_call | solution.py:421
  216.9 0.0 copy-done.1
  216.9 1.4 multiply_add_fusion
  218.3 0.0 copy-start
  218.3 1.9 copy.11
  220.3 0.0 copy-done
  220.3 0.8 copy.12
Async XLA Ops:
  0.6 216.3 %copy-start.1 = (f32[32,512]{1,0:T(8,128)S(1)}, f32[32,512]{1,0:T(8,128)}, u32[]{:S(2)}) copy-start(f32[32,512]{1,0:T(8,128)} %param.11) | copy-start | bytes 196612
  218.3 1.9 copy-start
where the time goes:
time: 221 us
  Pallas kernels  216 us (98%)
  local copies, waits for them, and re-layouts  2.74 us (1%)
    pallas_call x1, Pallas kernels, per_device(): pl.pallas_call(functools.partial(kernel, n, T, B, Q), out_shape=(jax.Shap...  216 us

commit v1 on v0

v1 whole, which is shorter than its diff:
```python
import functools

import jax
import jax.numpy as jnp
from jax import lax
from jax.experimental import pallas as pl
from jax.experimental.pallas import tpu as pltpu
from jax.sharding import PartitionSpec as P

MESH = pl.DeviceIdType.MESH
F32 = jnp.float32
BF16 = jnp.bfloat16
B = 4
NX = 4
X_COLS = (256, 384, 256)
O_COLS = (256, 128)


def kernel(
    A, fwd, saved, cot, up, down, out, ing, gout,
    Xb, Wsrc, Wb, H, Pb, Rx0, Rx1, Ry0, Ry1, Sx0, Sx1, Sy0, Sy1, Rz0, Rz1, Rw0, Rw1,
    Gs, Gi, Gc, Gsend, Grecv, Gy,
    lx, lw, wyS, wyR, wS, wR, wcS, wcR, xaS, xaR, xbS, xbR, xcS, xcR,
    gcS, gcR, gS, gR, hS, hR, rxS, rxR, ryS, ryR, rzS, rzR, rwS, rwR, agS, agR, odS, odR,
):
    f, t = lax.axis_index("fs"), lax.axis_index("tp")
    z, p = lax.div(f, B), lax.rem(f, B)
    x, c = lax.div(t, 2), lax.rem(t, 2)
    rows, D = fwd.shape
    half = rows // 2
    Rw, F = up.shape
    Fs = F // B
    quarter = D // NX
    tokens = B * half
    per = A // NX

    peers = [lax.rem(p + i, B) for i in range(1, B)]
    mates = [lax.rem(x + i, NX) for i in range(1, NX)]

    def at_z(d):
        return lax.rem(z + (d + A), A)

    def dev_y(q):
        return (z * B + q, t)

    def dev_x(m):
        return (f, m * 2 + c)

    def dev_z(d):
        return (at_z(d) * B + p, t)

    partner = (f, x * 2 + (1 - c))
    me = (f, t)

    mine = pl.ds(pl.multiple_of(c * Fs, Fs), Fs)
    other = pl.ds(pl.multiple_of((1 - c) * Fs, Fs), Fs)
    my_rows = pl.ds(pl.multiple_of(c * half, half), half)
    its_rows = pl.ds(pl.multiple_of((1 - c) * half, half), half)

    def slice_of(q):
        return pl.ds(pl.multiple_of(q * Fs, Fs), Fs)

    acts = (fwd, saved, cot)
    own = []
    for pc, w in enumerate((up, down)):
        own.append(pltpu.make_async_copy(w, Wsrc.at[pc], lw.at[pc]))
        own.append(
            pltpu.make_async_copy(w.at[:, slice_of(p)], Wb.at[pc, z, p, :, mine], lw.at[2 + pc])
        )
    for j in (1, 2, 0):
        for k in range(NX):
            own.append(
                pltpu.make_async_copy(
                    acts[j].at[my_rows, pl.ds(k * quarter, quarter)], Xb.at[j, p, k], lx.at[j, k]
                )
            )
    for copy in own:
        copy.start()

    barrier = pltpu.get_barrier_semaphore()
    greeted = (
        [dev_y(q) for q in peers] + [dev_x(m) for m in mates] + [partner]
        + [dev_z(d) for d in (1, 2, -1, -2)]
    )
    for device in greeted:
        pl.semaphore_signal(barrier, inc=1, device_id=device, device_id_type=MESH)
    pl.semaphore_wait(barrier, len(greeted))
    for copy in own:
        copy.wait()

    started = []

    def send(src, dst, send_sem, recv_sem, device):
        copy = pltpu.make_async_remote_copy(
            src_ref=src, dst_ref=dst, send_sem=send_sem, recv_sem=recv_sem,
            device_id=device, device_id_type=MESH,
        )
        copy.start()
        started.append(copy)

    def arrived(ref, send_sem, recv_sem, device):
        pltpu.make_async_remote_copy(
            src_ref=ref, dst_ref=ref, send_sem=send_sem, recv_sem=recv_sem,
            device_id=device, device_id_type=MESH,
        ).wait_recv()

    for i, q in enumerate(peers):
        send(
            Wsrc.at[:, :, slice_of(q)], Wb.at[:, z, p, :, mine], wyS.at[i], wyR.at[p], dev_y(q)
        )

    def block(z0, q):
        return Wb.at[:, z0, q, :, mine]

    order = [p] + peers

    def relay(s, d, i):
        way = 1 if s == 0 else -1
        z0, q = at_z(-way * d), order[i]
        for hop in (2, 1):
            if d + hop == A // 2 and (i < B // 2) != (s == 0):
                continue
            send(
                block(z0, q), block(z0, q), wS.at[s, d // 2, i, hop - 1], wR.at[z0, q],
                dev_z(way * hop),
            )

    def w_arrived(z0, q):
        arrived(block(z0, q), wS.at[0, 0, 0, 0], wR.at[z0, q], me)

    for s in range(2):
        relay(s, 0, 0)

    def quarter_part(j, q, m):
        return Xb.at[j, q, m, :, pl.ds(0, X_COLS[j])]

    def rest_part(j, q):
        return Xb.at[j, q, :, :, pl.ds(X_COLS[j], quarter - X_COLS[j])]

    for j in (1, 2, 0):
        for i, q in enumerate(peers):
            send(quarter_part(j, p, x), quarter_part(j, p, x), xaS.at[j, i], xaR.at[j, p], dev_y(q))
    for j in (1, 2, 0):
        for i, q in enumerate(peers):
            send(rest_part(j, p), rest_part(j, p), xbS.at[j, i], xbR.at[j, p], dev_y(q))

    for i, q in enumerate(peers):
        arrived(Wb.at[:, z, q, :, mine], wyS.at[i], wyR.at[q], me)
        for s in range(2):
            relay(s, 0, 1 + i)

    def to_partner(z0):
        there = Wb.at[:, z0, :, :, mine]
        send(there, there, wcS.at[z0], wcR.at[z0], partner)

    to_partner(z)

    def act_share(j):
        for i, q in enumerate(peers):
            arrived(quarter_part(j, q, x), xaS.at[j, i], xaR.at[j, q], me)
            for o, m in enumerate(mates):
                send(
                    quarter_part(j, q, x), quarter_part(j, q, x),
                    xcS.at[j, i, o], xcR.at[j, q, x], dev_x(m),
                )

    def w_round(d):
        for i in range(B):
            for s in range(2):
                way = 1 if s == 0 else -1
                w_arrived(at_z(-way * d), order[i])
                relay(s, d, i)
        for e in (d, d - 1):
            for s in range(2):
                z0 = at_z(-(1 if s == 0 else -1) * e)
                if e != d:
                    for i in range(B):
                        w_arrived(z0, order[i])
                to_partner(z0)

    act_share(1)
    w_round(2)
    act_share(2)
    act_share(0)
    for d in range(4, A // 2, 2):
        w_round(d)
    for e in (A // 2 - 1, 1 - A // 2, A // 2):
        z0 = at_z(e)
        for i in range(B):
            w_arrived(z0, order[i])
        to_partner(z0)

    def act_arrived(j):
        for i, q in enumerate(peers):
            arrived(rest_part(j, q), xbS.at[j, i], xbR.at[j, q], me)
            for o, m in enumerate(mates):
                arrived(quarter_part(j, q, m), xcS.at[j, i, o], xcR.at[j, q, m], me)

    act_arrived(1)
    act_arrived(2)
    for e in range(A):
        there = Wb.at[:, e, :, :, other]
        arrived(there, wcS.at[e], wcR.at[e], me)

    def weights(pc, k):
        return Wb[pc, k * per:(k + 1) * per].reshape(quarter, 2 * Fs)

    def product(j, pc):
        total = jnp.zeros((tokens, 2 * Fs), F32)
        for k in range(NX):
            total += jnp.dot(
                Xb[j, :, k].reshape(tokens, quarter), weights(pc, k), preferred_element_type=F32
            )
        return total

    pre = product(1, 0)
    d_hidden = product(2, 1)
    H[1] = (d_hidden * 2.0 * jnp.maximum(pre, 0.0)).astype(BF16)
    turned = jnp.concatenate([H[1, :, other], H[1, :, mine]], axis=1)
    depth = D // A
    for k in range(NX):
        term = lax.dot_general(
            Xb[1, :, k].reshape(tokens, quarter), turned,
            (((0,), (0,)), ((), ())), preferred_element_type=F32,
        )
        group = pl.ds(k * per, per)
        Gs[group] = term[:, :Fs].astype(BF16).reshape(per, depth, Fs)
        Gc[group] = term[:, Fs:].reshape(per, depth, Fs)
        send(Gs.at[group], Gi.at[group], gcS.at[k], gcR.at[k], partner)

    Rx, Ry, Sx, Sy, Rz, Rq = (Rx0, Rx1), (Ry0, Ry1), (Sx0, Sx1), (Sy0, Sy1), (Rz0, Rz1), (Rw0, Rw1)

    def spread(o, pc):
        for k in range(NX):
            part = lax.dot_general(
                H[o], weights(pc, k), (((1,), (1,)), ((), ())), preferred_element_type=F32
            )
            Pb[o, :, k] = part.astype(BF16).reshape(B, half, quarter)
        v = O_COLS[o]
        for i, m in enumerate(mates):
            send(
                Pb.at[o, :, m, :, pl.ds(0, v)], Rx[o].at[x], rxS.at[o, i], rxR.at[o, x], dev_x(m)
            )
        for i, q in enumerate(peers):
            send(
                Pb.at[o, q, :, :, pl.ds(v, quarter - v)], Ry[o].at[p], ryS.at[o, i], ryR.at[o, p],
                dev_y(q),
            )

    spread(1, 0)

    def g_send(s, d, value):
        way = 1 if s == 0 else -1
        hop = 1 if d % 2 else 2
        Gsend[s, d - 1] = value.astype(BF16)
        send(
            Gsend.at[s, d - 1], Grecv.at[s, d - 1], gS.at[s, d - 1], gR.at[s, d - 1],
            dev_z(way * hop),
        )

    def g_mine(e):
        at = at_z(e)
        return Gc[at] + Gi[at].astype(F32)

    def g_got(s, d):
        arrived(Grecv.at[s, d - 1], gS.at[s, d - 1], gR.at[s, d - 1], me)
        return Grecv[s, d - 1].astype(F32)

    for k in range(NX):
        group = pl.ds(k * per, per)
        arrived(Gi.at[group], gcS.at[k], gcR.at[k], me)
    far = A // 2
    g_send(0, far, g_mine(far))
    for d in range(far - 1, 0, -2):
        for s in range(2):
            g_send(s, d, g_mine(d if s == 0 else -d))

    act_arrived(0)
    positive = jnp.maximum(product(0, 0), 0.0)
    H[0] = (positive * positive).astype(BF16)
    spread(0, 1)

    def g_round(d):
        for s in range(2):
            value = g_mine(d if s == 0 else -d) + g_got(s, d + 1)
            if s == 0 or d + 2 < far:
                value = value + g_got(s, d + 2)
            g_send(s, d, value)

    def x_sums(o):
        v = O_COLS[o]
        for i, m in enumerate(mates):
            arrived(Rx[o].at[m], rxS.at[o, i], rxR.at[o, m], me)
        for i, q in enumerate(peers + [p]):
            total = Pb[o, q, x, :, :v].astype(F32)
            for m in mates:
                total = total + Rx[o][m, q].astype(F32)
            Sx[o][q] = total.astype(BF16)
            if i < len(peers):
                send(Sx[o].at[q], Rz[o].at[p], rzS.at[o, i], rzR.at[o, p], dev_y(q))

    def y_sums(o):
        v = O_COLS[o]
        for i, q in enumerate(peers):
            arrived(Ry[o].at[q], ryS.at[o, i], ryR.at[o, q], me)
        for i, m in enumerate(mates + [x]):
            total = Pb[o, p, m, :, v:].astype(F32)
            for q in peers:
                total = total + Ry[o][q, m].astype(F32)
            Sy[o][m] = total.astype(BF16)
            if i < len(mates):
                send(Sy[o].at[m], Rq[o].at[x], rwS.at[o, i], rwR.at[o, x], dev_x(m))

    outs = (out, ing)

    def piece(o, m, which):
        return outs[o].at[which, pl.ds(pl.multiple_of(m * quarter, quarter), quarter)]

    def finish(o):
        v = O_COLS[o]
        for i, q in enumerate(peers):
            arrived(Rz[o].at[q], rzS.at[o, i], rzR.at[o, q], me)
        total = Sx[o][p].astype(F32)
        for q in peers:
            total = total + Rz[o][q].astype(F32)
        left = total.astype(BF16)
        for i, m in enumerate(mates):
            arrived(Rq[o].at[m], rwS.at[o, i], rwR.at[o, m], me)
        total = Sy[o][x].astype(F32)
        for m in mates:
            total = total + Rq[o][m].astype(F32)
        outs[o][my_rows, pl.ds(pl.multiple_of(x * quarter, quarter), quarter)] = jnp.concatenate(
            [left, total.astype(BF16)], axis=1
        )
        for i, m in enumerate(mates):
            send(piece(o, x, my_rows), piece(o, x, my_rows), agS.at[o, i], agR.at[o, x], dev_x(m))
        send(piece(o, x, my_rows), piece(o, x, my_rows), odS.at[o, x], odR.at[o, x], partner)

    def pass_on(o):
        for i, m in enumerate(mates):
            arrived(piece(o, m, my_rows), agS.at[o, i], agR.at[o, m], me)
            send(piece(o, m, my_rows), piece(o, m, my_rows), odS.at[o, m], odR.at[o, m], partner)

    g_round(6)
    x_sums(1)
    y_sums(1)
    g_round(4)
    x_sums(0)
    y_sums(0)
    g_round(2)
    finish(1)

    total = g_mine(0)
    for s in range(2):
        for d in (1, 2):
            total = total + g_got(s, d)
    Gy[...] = total.astype(BF16).reshape(B, Rw, Fs)
    for i, q in enumerate(peers):
        send(Gy.at[q], gout.at[:, slice_of(p)], hS.at[i], hR.at[p], dev_y(q))
    gout[:, slice_of(p)] = Gy[p]

    finish(0)
    pass_on(1)
    pass_on(0)
    for i, q in enumerate(peers):
        arrived(gout.at[:, slice_of(q)], hS.at[i], hR.at[q], me)
    for o in (1, 0):
        for m in range(NX):
            arrived(piece(o, m, its_rows), odS.at[o, m], odR.at[o, m], me)
    for copy in started:
        copy.wait_send()


def per_device(n, T, fwd_input, saved_input, out_cotangent, up_weight, down_weight, up_grad_sum):
    rows, D = fwd_input.shape
    Rw, F = up_weight.shape
    A = n // B
    Fs, half, quarter, depth = F // B, rows // 2, D // NX, D // A
    dma = pltpu.SemaphoreType.DMA
    flops = 12 * B * half * 2 * Fs * D
    anywhere = pl.BlockSpec(memory_space=pl.ANY)
    vmem = pl.BlockSpec(memory_space=pltpu.VMEM)
    v = O_COLS
    u = tuple(quarter - w for w in v)

    def pair(*shapes):
        return [pltpu.VMEM(shape, BF16) for shape in shapes]

    layer_out, input_grad, grad = pl.pallas_call(
        functools.partial(kernel, A),
        out_shape=(
            jax.ShapeDtypeStruct((rows, D), BF16),
            jax.ShapeDtypeStruct((rows, D), BF16),
            jax.ShapeDtypeStruct((Rw, F), BF16),
        ),
        in_specs=[anywhere] * 5,
        out_specs=(vmem,) * 3,
        scratch_shapes=[
            pltpu.VMEM((3, B, NX, half, quarter), BF16),
            pltpu.VMEM((2, Rw, F), BF16),
            pltpu.VMEM((2, A, B, Rw, 2 * Fs), BF16),
            pltpu.VMEM((2, B * half, 2 * Fs), BF16),
            pltpu.VMEM((2, B, NX, half, quarter), BF16),
            *pair((NX, B, half, v[0]), (NX, B, half, v[1])),
            *pair((B, NX, half, u[0]), (B, NX, half, u[1])),
            *pair((B, half, v[0]), (B, half, v[1])),
            *pair((NX, half, u[0]), (NX, half, u[1])),
            *pair((B, half, v[0]), (B, half, v[1])),
            *pair((NX, half, u[0]), (NX, half, u[1])),
            pltpu.VMEM((A, depth, Fs), BF16),
            pltpu.VMEM((A, depth, Fs), BF16),
            pltpu.VMEM((A, depth, Fs), F32),
            pltpu.VMEM((2, A // 2, depth, Fs), BF16),
            pltpu.VMEM((2, A // 2, depth, Fs), BF16),
            pltpu.VMEM((B, Rw, Fs), BF16),
            dma((3, NX)), dma((4,)),
            dma((B - 1,)), dma((B,)),
            dma((2, A // 4, B, 2)), dma((A, B)),
            dma((A,)), dma((A,)),
            dma((3, B - 1)), dma((3, B)),
            dma((3, B - 1)), dma((3, B)),
            dma((3, B - 1, NX - 1)), dma((3, B, NX)),
            dma((NX,)), dma((NX,)),
            dma((2, A // 2)), dma((2, A // 2)),
            dma((B - 1,)), dma((B,)),
            dma((2, NX - 1)), dma((2, NX)),
            dma((2, B - 1)), dma((2, B)),
            dma((2, B - 1)), dma((2, B)),
            dma((2, NX - 1)), dma((2, NX)),
            dma((2, NX - 1)), dma((2, NX)),
            dma((2, NX)), dma((2, NX)),
        ],
        compiler_params=pltpu.CompilerParams(
            collective_id=0, has_side_effects=True, vmem_limit_bytes=58 * 2**20
        ),
        cost_estimate=pl.CostEstimate(flops=flops, bytes_accessed=2**25, transcendentals=0),
    )(fwd_input, saved_input, out_cotangent, up_weight, down_weight.T)
    grad_part = grad.astype(F32)
    grad_scale = float(rows * n) ** (-0.5)
    return (layer_out, input_grad, up_grad_sum + grad_part * grad_scale)


def solution(mesh):
    placed = (
        P("fs", None),
        P("fs", None),
        P("fs", None),
        P("fs", "tp"),
        P("tp", "fs"),
        P("fs", "tp"),
    )
    return jax.shard_map(
        functools.partial(per_device, mesh.shape["fs"], mesh.shape["tp"]),
        mesh=mesh,
        in_specs=placed,
        out_specs=(P("fs", None), P("fs", None), P("fs", "tp")),
        check_vma=False,
    )
```

time: 221 us -> 77.3 us (0.35)
  Pallas kernels: 216 us -> 72.3 us
    pallas_call x1, Pallas kernels: 216 us -> 72.3 us  [per_device(): pl.pallas_call(functools.partial(kernel, A), out_shape=(jax.ShapeDtypeStr...]
where the time goes in v1:
time: 77.3 us; the launch traced here: 77 us
  Pallas kernels  72.3 us (94%)
  local copies, waits for them, and re-layouts  2.74 us (4%)
  other arithmetic  1.4 us (2%)
    pallas_call x1, Pallas kernels, per_device(): pl.pallas_call(functools.partial(kernel, A), out_shape=(jax.ShapeDtypeStr...  72.3 us
    unnamed x6, local copies, waits for them, and re-layouts  2.74 us

profile of v1, /device:TPU:1, one launch (start us, length us, event | category | flops | bytes accessed | tf_op | source)
XLA Modules:
  0.0 77.0 jit_solution(9220729700808575800)
XLA Ops:
  0.6 0.0 copy-start.1
  0.6 72.3 %shard_map.85 = (bf16[128,2048]{1,0:T(8,128)(2,1)}, bf16[128,2048]{1,0:T(8,128)(2,1)}, bf16[32,512]{1,0:T(8,128)(2,1)}) custom-call(bf16[128,2048]{1,0:T(8,128)(2,1)} %fwd.1, bf16[128,2048]{1,0:T(8,128)(2,1)} %saved.1, bf16[128,2048]{1,0:T(8,128)(2,1)} %cot.1, bf16[32,512]{1,0:T(8,128)(2,1)} %up.1, bf16[32,512]{1,0:T(8,128)(2,1)} %bitcast.1), custom_call_target="tpu_custom_call" | custom-call | flops 1610612736 | bytes 33554432 | tf_op jit(solution)/shard_map/pallas_call | solution.py:389
  72.9 0.0 copy-done.1
  72.9 1.4 %multiply_add_fusion = f32[32,512]{1,0:T(8,128)} fusion(f32[32,512]{1,0:T(8,128)S(1)} %copy-done.1, bf16[32,512]{1,0:T(8,128)(2,1)} %get-tuple-element.8), kind=kLoop, calls=%fused_computation | loop fusion | flops 49152 | bytes 163840 | tf_op jit(solution)/shard_map/add | solution.py:440
  74.3 0.0 copy-start
  74.3 1.9 %copy.11 = bf16[128,2048]{1,0:T(8,128)(2,1)} copy(bf16[128,2048]{1,0:T(8,128)(2,1)} %get-tuple-element.12) | data formatting | bytes 1048576
  76.2 0.0 copy-done
  76.3 0.8 %copy.12 = bf16[128,2048]{1,0:T(8,128)(2,1)} copy(bf16[128,2048]{1,0:T(8,128)(2,1)S(1)} %copy-done) | data formatting | bytes 1048576
Async XLA Ops:
  0.6 72.3 %copy-start.1 = (f32[32,512]{1,0:T(8,128)S(1)}, f32[32,512]{1,0:T(8,128)}, u32[]{:S(2)}) copy-start(f32[32,512]{1,0:T(8,128)} %param.11) | copy-start | bytes 196612
  74.3 1.9 %copy-start = (bf16[128,2048]{1,0:T(8,128)(2,1)S(1)}, bf16[128,2048]{1,0:T(8,128)(2,1)}, u32[]{:S(2)}) copy-start(bf16[128,2048]{1,0:T(8,128)(2,1)} %get-tuple-element.13) | copy-start | bytes 1572868
